TPU v7x, 32 devices: a whole 2x2x4 slice. The times are simulated.
32 devices in a mesh: grp: 2 (over y), fs: 4 (over z), tp: 4 (over x, core).
Axes of the slice: x: 2, y: 2, z: 4, core: 2. Of those that a mesh axis runs over, the one named last changes fastest.
Arguments:
- tokens: bfloat16 [4096, 2048], P(('grp', 'fs')), parts along dimension 0, may hold values from -6 to 6
- norm_in: bfloat16 [2048], replicated, may hold values from 0.099609375 to 1.8984375
- w_value: bfloat16 [2048, 2048], P('fs', 'tp'), may hold values from -0.125 to 0.125
- w_gate: bfloat16 [2048, 2048], P('fs', 'tp'), may hold values from -0.125 to 0.125
- conv_kernel: float32 [31, 2048], replicated, as said below
- ln_gain: bfloat16 [2048], replicated, may hold values from 0.099609375 to 1.8984375
- ln_shift: bfloat16 [2048], replicated, may hold values from -3 to 3
- w_out: bfloat16 [2048, 2048], P('tp', 'fs'), may hold values from -0.125 to 0.125
- norm_mlp: bfloat16 [2048], replicated, may hold values from 0.099609375 to 1.8984375
- w_up: bfloat16 [2048, 8192], P('fs', 'tp'), may hold values from -0.125 to 0.125
- w_down: bfloat16 [8192, 2048], P('tp', 'fs'), may hold values from -0.0625 to 0.0625
Outputs:
- layer_out: bfloat16 [4096, 2048], P(('grp', 'fs', 'tp')), parts along dimension 0
There are 2 independent parts, one for each index of `grp`. A program takes and returns all parts, laid end to end along the dimension named above; an argument that names none is the same for every part. Nothing has to cross between parts.
Inputs may be any that keep to these rules, and one draw needn't show every extreme that they name: `conv_kernel`: a depthwise kernel.
All inputs are finite; a program needn't handle non-finite values.
Results may differ from a plain program's by a relative error of at most 0.018.
Values may be sent and summed in bfloat16 or wider, within the bound.
A program may use at most 64 MiB of HBM per device.

v0:
```python
import jax
import jax.numpy as jnp
from jax import lax
from jax.sharding import PartitionSpec as P

D = 2048
KERNEL = 31


def rms_scale(values, gain):
    as_float = values.astype(jnp.float32)
    scaled = as_float * lax.rsqrt(jnp.mean(as_float * as_float, axis=-1, keepdims=True) + 1e-06)
    return scaled * gain.astype(jnp.float32)


def shards(
    tokens, norm_in, w_value, w_gate, conv_kernel, ln_gain, ln_shift, w_out, norm_mlp, w_up, w_down
):
    seq_len = tokens.shape[0]
    col_width = w_value.shape[1]
    offset = lax.axis_index("tp") * col_width
    row_share = seq_len // lax.axis_size("tp")
    own_start = lax.axis_index("tp") * row_share
    normed_in = rms_scale(tokens, norm_in).astype(jnp.bfloat16)
    columns = normed_in
    values_f = jnp.dot(
        columns,
        lax.all_gather(w_value, "fs", axis=0, tiled=True),
        preferred_element_type=jnp.float32,
    )
    gate_act = jnp.dot(
        columns,
        lax.all_gather(w_gate, "fs", axis=0, tiled=True),
        preferred_element_type=jnp.float32,
    )
    gated = values_f * jax.nn.sigmoid(gate_act)
    kernel = lax.dynamic_slice_in_dim(conv_kernel, offset, col_width, 1)
    padded = jnp.pad(gated, ((KERNEL - 1, 0), (0, 0)))
    convolved = jnp.zeros_like(gated)
    for tap_index in range(KERNEL):
        convolved = convolved + kernel[tap_index][None, :] * padded[tap_index : tap_index + seq_len]
    stats = lax.psum((jnp.sum(convolved, axis=1), jnp.sum(convolved * convolved, axis=1)), "tp")
    chan_mean = (stats[0] / D)[:, None]
    chan_msq = (stats[1] / D)[:, None]
    variance = chan_msq - chan_mean * chan_mean
    gain_part = lax.dynamic_slice_in_dim(ln_gain, offset, col_width, 0).astype(jnp.float32)
    shift_part = lax.dynamic_slice_in_dim(ln_shift, offset, col_width, 0).astype(jnp.float32)
    normed = (convolved - chan_mean) * lax.rsqrt(variance + 1e-05) * gain_part + shift_part
    activated = jax.nn.silu(normed).astype(jnp.bfloat16)
    partial_value = jnp.dot(
        activated,
        lax.all_gather(w_out, "fs", axis=1, tiled=True),
        preferred_element_type=jnp.float32,
    )
    mixed = lax.psum(partial_value.astype(jnp.bfloat16), "tp").astype(jnp.float32)
    residual = tokens.astype(jnp.float32) + mixed
    normed_mlp = rms_scale(residual, norm_mlp).astype(jnp.bfloat16)
    residual_own = lax.dynamic_slice_in_dim(residual, own_start, row_share, 0)
    columns = normed_mlp
    up_act = jnp.dot(
        columns, lax.all_gather(w_up, "fs", axis=0, tiled=True), preferred_element_type=jnp.float32
    )
    hidden = jnp.square(jax.nn.relu(up_act)).astype(jnp.bfloat16)
    whole_down = lax.all_gather(w_down, "fs", axis=1, tiled=True)
    mlp_own = lax.psum_scatter(
        jnp.dot(hidden, whole_down, preferred_element_type=jnp.float32).astype(jnp.bfloat16),
        "tp",
        scatter_dimension=0,
        tiled=True,
    ).astype(jnp.float32)
    return (residual_own + mlp_own).astype(jnp.bfloat16)


def solution(mesh):
    in_specs = (
        P(("grp", "fs"), None),
        P(),
        P("fs", "tp"),
        P("fs", "tp"),
        P(),
        P(),
        P(),
        P("tp", "fs"),
        P(),
        P("fs", "tp"),
        P("tp", "fs"),
    )
    out_specs = P(("grp", "fs", "tp"), None)
    return jax.shard_map(shards, mesh=mesh, in_specs=in_specs, out_specs=out_specs, check_vma=False)
```

profile of v0, /device:TPU:0, one launch (start us, length us, event | category | flops | bytes accessed | tf_op | source)
XLA Modules:
  0.0 559.9 jit_solution(14983291080787817863)
XLA Ops:
  6.5 0.0 copy-start
  6.5 0.0 all-gather.8.cloned.1.call-start
  6.5 0.7 all-gather.8.cloned.1.call-update
  7.3 0.0 all-gather.6.cloned.1.call-start
  7.3 0.7 all-gather.6.cloned.1.call-update
  8.0 0.0 all-gather.10.cloned.1.call-start
  8.1 0.7 all-gather.10.cloned.1.call-update
  8.7 0.0 all-reduce.4.cloned.1.call-start
  8.8 0.7 convert_element_type.46
  9.5 0.8 dynamic-slice_convert_fusion
  10.3 1.1 fusion.50
  11.4 1.4 constant_dynamic-slice_fusion
  12.8 2.1 fusion
  14.8 42.5 %all-gather.8.cloned.1.call-done = bf16[2048,512]{1,0:T(8,128)(2,1)} async-done(((bf16[512,512]{1,0:T(8,128)(2,1)}), bf16[2048,512]{1,0:T(8,128)(2,1)}) %all-gather.8.cloned.1.call-update) | async-done | bytes 2097168 | tf_op jit(solution)/shard_map/all_gather | solution.py:33
  57.3 0.0 copy-done
  57.3 3.0 fusion.7
  60.4 43.0 %all-gather.6.cloned.1.call-done = bf16[2048,512]{1,0:T(8,128)(2,1)} async-done(((bf16[512,512]{1,0:T(8,128)(2,1)}), bf16[2048,512]{1,0:T(8,128)(2,1)}) %all-gather.6.cloned.1.call-update) | async-done | bytes 2097168 | tf_op jit(solution)/shard_map/all_gather | solution.py:28
  103.4 2.9 convolution_multiply_fusion
  106.3 5.0 fusion.49
  111.3 6.8 %all-reduce.1 = (f32[512]{0:T(512)S(1)}, f32[512]{0:T(512)S(1)}) all-reduce(f32[512]{0:T(512)S(1)} %get-tuple-element.6, f32[512]{0:T(512)S(1)} %get-tuple-element.5), channel_id=1, replica_groups=mesh['grp'=2,'fs'=4,'tp'=4] {'tp'}, use_global_device_ids=true, to_apply=%region_4.5 | all-reduce | flops 1024 | bytes 8192 | tf_op jit(solution)/shard_map/psum | solution.py:42
  118.1 31.4 %all-gather.10.cloned.1.call-done = bf16[512,2048]{1,0:T(8,128)(2,1)} async-done(((bf16[512,512]{1,0:T(8,128)(2,1)}), bf16[512,2048]{1,0:T(8,128)(2,1)}) %all-gather.10.cloned.1.call-update) | async-done | bytes 2097168 | tf_op jit(solution)/shard_map/all_gather | solution.py:52
  149.4 4.4 convolution_convert_fusion.1
  153.9 0.0 all-reduce.4.cloned.1.call-update
  153.9 0.0 copy-start.1
  153.9 0.0 all-gather.12.cloned.1.call-start
  153.9 0.5 all-gather.12.cloned.1.call-update
  154.5 0.0 all-gather.14.cloned.1.call-start
  154.5 0.5 all-gather.14.cloned.1.call-update
  155.1 0.2 reduce-scatter.2.cloned.1.call-start
  155.3 0.0 copy-done.1
  155.3 48.9 %all-reduce.4.cloned.1.call-done = bf16[512,2048]{1,0:T(8,128)(2,1)} async-done(((bf16[512,2048]{1,0:T(8,128)(2,1)}), bf16[512,2048]{1,0:T(8,128)(2,1)}) %all-reduce.4.cloned.1.call-update) | async-done | bytes 2097168 | tf_op jit(solution)/shard_map/psum | solution.py:55
  204.2 4.2 convert_add_fusion
  208.4 146.9 %all-gather.12.cloned.1.call-done = bf16[2048,2048]{1,0:T(8,128)(2,1)} async-done(((bf16[512,2048]{1,0:T(8,128)(2,1)}), bf16[2048,2048]{1,0:T(8,128)(2,1)}) %all-gather.12.cloned.1.call-update) | async-done | bytes 8388624 | tf_op jit(solution)/shard_map/all_gather | solution.py:61
  355.4 149.3 %all-gather.14.cloned.1.call-done = bf16[2048,2048]{1,0:T(8,128)(2,1)} async-done(((bf16[2048,512]{1,0:T(8,128)(2,1)}), bf16[2048,2048]{1,0:T(8,128)(2,1)}) %all-gather.14.cloned.1.call-update) | async-done | bytes 8388624 | tf_op jit(solution)/shard_map/all_gather | solution.py:64
  504.6 16.6 %convolution_convert_fusion = bf16[512,2048]{1,0:T(8,128)(2,1)} fusion(bf16[2048,2048]{1,0:T(8,128)(2,1)} %all-gather.14.cloned.1.call-done, bf16[2048,2048]{1,0:T(8,128)(2,1)} %all-gather.12.cloned.1.call-done, f32[2048]{0:T(1024)S(1)} %convert_element_type.53, f32[512]{0:T(512)S(1)} %add_rsqrt_fusion, bf16[512,2048]{1,0:T(8,128)(2,1)S(1)} %copy-done, ...), kind=kOutput, calls=%fused_computation.9 | convolution fusion | flops 8600420352 | bytes 23078912 | tf_op jit(solution)/shard_map/dot_general | solution.py:66
  521.2 0.0 reduce-scatter.2.cloned.1.call-update
  521.2 29.5 %reduce-scatter.2.cloned.1.call-done = bf16[128,2048]{1,0:T(8,128)(2,1)} async-done(((bf16[512,2048]{1,0:T(8,128)(2,1)}), bf16[128,2048]{1,0:T(8,128)(2,1)}) %reduce-scatter.2.cloned.1.call-update) | async-done | bytes 524304 | tf_op jit(solution)/shard_map/reduce_scatter | solution.py:65
  550.8 2.3 add_convert_fusion
  (4 shorter events, 0.0 us)
Async XLA Ops:
  6.5 50.8 %copy-start = (bf16[512,2048]{1,0:T(8,128)(2,1)S(1)}, bf16[512,2048]{1,0:T(8,128)(2,1)}, u32[]{:S(2)}) copy-start(bf16[512,2048]{1,0:T(8,128)(2,1)} %param.11) | copy-start | bytes 6291460
  6.5 50.8 %all-gather.8.cloned.1.call-start = ((), (), s32[]{:S(2)}) async-start(), calls=%async_computation.2 | async-start | bytes 2621440 | tf_op jit(solution)/shard_map/all_gather | solution.py:33
  7.3 96.1 %all-gather.6.cloned.1.call-start = ((), (), s32[]{:S(2)}) async-start(), calls=%async_computation.1 | async-start | bytes 2621440 | tf_op jit(solution)/shard_map/all_gather | solution.py:28
  8.0 141.4 %all-gather.10.cloned.1.call-start = ((), (), s32[]{:S(2)}) async-start(), calls=%async_computation.3 | async-start | bytes 2621440 | tf_op jit(solution)/shard_map/all_gather | solution.py:52
  8.7 195.5 %all-reduce.4.cloned.1.call-start = ((), (), s32[]{:S(2)}) async-start(), calls=%async_computation.4 | async-start | bytes 4194304 | tf_op jit(solution)/shard_map/psum | solution.py:55
  153.9 1.4 copy-start.1
  153.9 201.5 %all-gather.12.cloned.1.call-start = ((), (), s32[]{:S(2)}) async-start(), calls=%async_computation.5 | async-start | bytes 10485760 | tf_op jit(solution)/shard_map/all_gather | solution.py:61
  154.5 350.1 %all-gather.14.cloned.1.call-start = ((), (), s32[]{:S(2)}) async-start(), calls=%async_computation.6 | async-start | bytes 10485760 | tf_op jit(solution)/shard_map/all_gather | solution.py:64
  155.1 395.7 %reduce-scatter.2.cloned.1.call-start = ((), (), s32[]{:S(2)}) async-start(), calls=%async_computation.7 | async-start | bytes 2621440 | tf_op jit(solution)/shard_map/reduce_scatter | solution.py:65
Sparse Core Ops, SparseCore 0:
  8.9 48.3 all-gather.7
  58.9 44.4 all-gather.5
  105.0 44.4 all-gather.9
  154.0 50.1 all-reduce.3
  205.6 149.6 all-gather.11
  356.8 147.7 all-gather.13
  521.4 29.3 reduce-scatter.1
where the time goes:
time: 560 us
  waiting for transfers between devices  495 us (88%)
  matrix products  26.9 us (5%)
  other arithmetic  15 us (3%)
  between operations  13.6 us (2%)
  blocking collectives  6.79 us (1%)
    all_gather x1, waiting for transfers between devices, shards(): whole_down = lax.all_gather(w_down, 'fs', axis=1, tiled=True)  149 us
    all_gather x1, waiting for transfers between devices, shards(): lax.all_gather(w_up, 'fs', axis=0, tiled=True)  147 us
    psum x1, waiting for transfers between devices, shards(): lax.psum(partial_value.astype(jnp.bfloat16), 'tp').astype(jnp.float32)  48.9 us
    all_gather x1, waiting for transfers between devices, shards(): lax.all_gather(w_value, 'fs', axis=0, tiled=True)  43 us
    all_gather x1, waiting for transfers between devices, shards(): lax.all_gather(w_gate, 'fs', axis=0, tiled=True)  42.5 us
    all_gather x1, waiting for transfers between devices, shards(): lax.all_gather(w_out, 'fs', axis=1, tiled=True)  31.4 us
    reduce_scatter x1, waiting for transfers between devices, shards(): lax.psum_scatter(jnp.dot(hidden, whole_down, preferred_element_type=jnp.f...  29.5 us
    dot_general x1, matrix products, shards(): jnp.dot(hidden, whole_down, preferred_element_type=jnp.float32)  16.6 us
  transfers between devices with their start and end apart: 7, of which 7 were waited for; matrix products, arithmetic and copies ran while one was open for 4% of the time, Pallas kernels for 0%

commit v1 on v0

--- a/solution.py
+++ b/solution.py
@@ -5,6 +5,17 @@
 
 D = 2048
 KERNEL = 31
+
+
+def turned_line(shard, axis, dim):
+    size = lax.axis_size(axis)
+    right = [(i, (i + 1) % size) for i in range(size)]
+    pieces = [shard]
+    for stride in range(1, size):
+        pieces = [lax.ppermute(pieces[0], axis, right), *pieces]
+    whole = jnp.concatenate(pieces, axis=dim)
+    shift = (lax.axis_index(axis) + 1) * pieces[-1].shape[dim]
+    return jnp.roll(whole, shift, axis=dim)
 
 
 def rms_scale(values, gain):
@@ -61,7 +72,7 @@
         columns, lax.all_gather(w_up, "fs", axis=0, tiled=True), preferred_element_type=jnp.float32
     )
     hidden = jnp.square(jax.nn.relu(up_act)).astype(jnp.bfloat16)
-    whole_down = lax.all_gather(w_down, "fs", axis=1, tiled=True)
+    whole_down = turned_line(w_down, "fs", 1)
     mlp_own = lax.psum_scatter(
         jnp.dot(hidden, whole_down, preferred_element_type=jnp.float32).astype(jnp.bfloat16),
         "tp",

time: 560 us -> 505 us (0.902)
  waiting for transfers between devices: 495 us -> 392 us
  starting transfers between devices: 0.42 us -> 27.6 us
  local copies, waits for them, and re-layouts: 2.49 us -> 22.6 us
    ppermute x0 -> x3, waiting for transfers between devices: none -> 221 us  [turned_line(): pieces = [lax.ppermute(pieces[0], axis, right), *pieces]]
    all_gather x1 -> x0, waiting for transfers between devices: 149 us -> none  [shards(): whole_down = lax.all_gather(w_down, 'fs', axis=1, tiled=True)]
    all_gather x1, waiting for transfers between devices: 147 us -> 6.69 us  [shards(): lax.all_gather(w_up, 'fs', axis=0, tiled=True)]
    psum x1, waiting for transfers between devices: 48.9 us -> 0.01 us  [shards(): lax.psum(partial_value.astype(jnp.bfloat16), 'tp').astype(jnp.float32)]
    ppermute x0 -> x3, starting transfers between devices: none -> 27.4 us  [turned_line(): pieces = [lax.ppermute(pieces[0], axis, right), *pieces]]
    unnamed x4 -> x17, local copies, waits for them, and re-layouts: 0.01 us -> 18.6 us
    reduce_scatter x1, waiting for transfers between devices: 29.5 us -> 45.4 us  [shards(): lax.psum_scatter(jnp.dot(hidden, whole_down, preferred_element_type=jnp.f...]
  transfers between devices with their start and end apart: 7 -> 9, of which waited for: 7 -> 8; matrix products, arithmetic and copies ran while one was open for 4% -> 8% of each run, Pallas kernels for 0% -> 0%
where the time goes in v1:
time: 505 us
  waiting for transfers between devices  392 us (78%)
  starting transfers between devices  27.6 us (5%)
  matrix products  27.6 us (5%)
  local copies, waits for them, and re-layouts  22.6 us (4%)
  other arithmetic  15.1 us (3%)
  between operations  13.5 us (3%)
  blocking collectives  6.79 us (1%)
    ppermute x3, waiting for transfers between devices, turned_line(): pieces = [lax.ppermute(pieces[0], axis, right), *pieces]  221 us
    reduce_scatter x1, waiting for transfers between devices, shards(): lax.psum_scatter(jnp.dot(hidden, whole_down, preferred_element_type=jnp.f...  45.4 us
    all_gather x1, waiting for transfers between devices, shards(): lax.all_gather(w_gate, 'fs', axis=0, tiled=True)  42.5 us
    all_gather x1, waiting for transfers between devices, shards(): lax.all_gather(w_value, 'fs', axis=0, tiled=True)  42.4 us
    all_gather x1, waiting for transfers between devices, shards(): lax.all_gather(w_out, 'fs', axis=1, tiled=True)  31.4 us
    ppermute x3, starting transfers between devices, turned_line(): pieces = [lax.ppermute(pieces[0], axis, right), *pieces]  27.4 us
    unnamed x17, local copies, waits for them, and re-layouts  18.6 us
    dot_general x1, matrix products, shards(): jnp.dot(hidden, whole_down, preferred_element_type=jnp.float32)  16.5 us
  transfers between devices with their start and end apart: 9, of which 8 were waited for; matrix products, arithmetic and copies ran while one was open for 8% of the time, Pallas kernels for 0%

profile of v1, /device:TPU:0, one launch (start us, length us, event | category | flops | bytes accessed | tf_op | source)
XLA Modules:
  0.0 504.8 jit_solution(14855344243949360485)
XLA Ops:
  6.5 0.0 all-gather.7.cloned.1.call-start
  6.5 0.7 all-gather.7.cloned.1.call-update
  7.3 0.0 all-gather.5.cloned.1.call-start
  7.3 0.7 all-gather.5.cloned.1.call-update
  8.0 0.0 all-gather.9.cloned.1.call-start
  8.1 0.7 all-gather.9.cloned.1.call-update
  8.7 0.0 all-reduce.4.cloned.1.call-start
  8.8 0.7 convert_element_type.46
  9.5 0.8 dynamic-slice_convert_fusion
  10.3 1.1 fusion.57
  11.4 1.4 constant_dynamic-slice_fusion
  12.7 2.1 fusion.2
  14.8 0.0 copy-start
  14.8 42.5 %all-gather.7.cloned.1.call-done = bf16[2048,512]{1,0:T(8,128)(2,1)} async-done(((bf16[512,512]{1,0:T(8,128)(2,1)}), bf16[2048,512]{1,0:T(8,128)(2,1)}) %all-gather.7.cloned.1.call-update) | async-done | bytes 2097168 | tf_op jit(solution)/shard_map/all_gather | solution.py:44
  57.3 3.7 fusion.12
  61.0 42.4 %all-gather.5.cloned.1.call-done = bf16[2048,512]{1,0:T(8,128)(2,1)} async-done(((bf16[512,512]{1,0:T(8,128)(2,1)}), bf16[2048,512]{1,0:T(8,128)(2,1)}) %all-gather.5.cloned.1.call-update) | async-done | bytes 2097168 | tf_op jit(solution)/shard_map/all_gather | solution.py:39
  103.4 0.0 copy-done
  103.4 2.9 convolution_multiply_fusion
  106.3 5.0 fusion.56
  111.3 6.8 %all-reduce.1 = (f32[512]{0:T(512)S(1)}, f32[512]{0:T(512)S(1)}) all-reduce(f32[512]{0:T(512)S(1)} %get-tuple-element.6, f32[512]{0:T(512)S(1)} %get-tuple-element.5), channel_id=1, replica_groups=mesh['grp'=2,'fs'=4,'tp'=4] {'tp'}, use_global_device_ids=true, to_apply=%region_4.5 | all-reduce | flops 1024 | bytes 8192 | tf_op jit(solution)/shard_map/psum | solution.py:53
  118.1 31.4 %all-gather.9.cloned.1.call-done = bf16[512,2048]{1,0:T(8,128)(2,1)} async-done(((bf16[512,512]{1,0:T(8,128)(2,1)}), bf16[512,2048]{1,0:T(8,128)(2,1)}) %all-gather.9.cloned.1.call-update) | async-done | bytes 2097168 | tf_op jit(solution)/shard_map/all_gather | solution.py:63
  149.4 4.4 convolution_convert_fusion
  153.9 0.0 copy-start.4
  153.9 0.0 all-reduce.4.cloned.1.call-update
  153.9 0.0 all-gather.11.cloned.1.call-start
  154.0 0.5 all-gather.11.cloned.1.call-update
  154.5 0.0 reduce-scatter.2.cloned.1.call-start
  154.6 0.2 collective-permute-start
  154.8 49.0 %collective-permute-done = bf16[2048,512]{1,0:T(8,128)(2,1)S(1)} collective-permute-done((bf16[2048,512]{1,0:T(8,128)(2,1)}, bf16[2048,512]{1,0:T(8,128)(2,1)S(1)}, u32[]{:S(2)}, u32[]{:S(2)}) %collective-permute-start) | collective-permute-done | bytes 2097184 | tf_op jit(solution)/shard_map/ppermute | solution.py:15
  203.8 0.0 copy-start.2
  203.8 1.4 copy-done.2
  205.2 0.0 collective-permute-start.1
  205.2 84.0 %collective-permute-done.1 = bf16[2048,512]{1,0:T(8,128)(2,1)} collective-permute-done((bf16[2048,512]{1,0:T(8,128)(2,1)S(1)}, bf16[2048,512]{1,0:T(8,128)(2,1)}, u32[]{:S(2)}, u32[]{:S(2)}) %collective-permute-start.1) | collective-permute-done | bytes 2097184 | tf_op jit(solution)/shard_map/ppermute | solution.py:15
  289.3 27.2 %collective-permute-start.2 = (bf16[2048,512]{1,0:T(8,128)(2,1)}, bf16[2048,512]{1,0:T(8,128)(2,1)}, u32[]{:S(2)}, u32[]{:S(2)}) collective-permute-start(bf16[2048,512]{1,0:T(8,128)(2,1)} %collective-permute-done.1), channel_id=1, source_target_pairs={{0,4},{4,8},{8,12},{12,0},{1,5},{5,9},{9,13},{13,1},{2,6},{6,10},{... | collective-permute-start | bytes 6291464 | tf_op jit(solution)/shard_map/ppermute | solution.py:15
  316.4 0.0 copy-done.4
  316.4 0.0 all-reduce.4.cloned.1.call-done
  316.4 4.2 convert_add_fusion
  320.7 0.0 copy-start.3
  320.7 87.5 %collective-permute-done.2 = bf16[2048,512]{1,0:T(8,128)(2,1)} collective-permute-done((bf16[2048,512]{1,0:T(8,128)(2,1)}, bf16[2048,512]{1,0:T(8,128)(2,1)}, u32[]{:S(2)}, u32[]{:S(2)}) %collective-permute-start.2) | collective-permute-done | bytes 2097184 | tf_op jit(solution)/shard_map/ppermute | solution.py:15
  408.2 3.1 constant_dynamic-update-slice_fusion.7
  411.3 0.0 copy-start.1
  411.3 3.3 constant_dynamic-update-slice_fusion.6
  414.6 0.0 copy-done.3
  414.6 1.6 constant_dynamic-update-slice_fusion.5
  416.2 0.0 copy-done.1
  416.2 1.5 constant_dynamic-update-slice_fusion.4
  417.7 3.1 constant_dynamic-update-slice_fusion.3
  420.8 3.1 constant_dynamic-update-slice_fusion.2
  423.9 1.5 constant_dynamic-update-slice_fusion.1
  425.5 1.5 constant_dynamic-update-slice_fusion
  427.0 6.7 %all-gather.11.cloned.1.call-done = bf16[2048,2048]{1,0:T(8,128)(2,1)} async-done(((bf16[512,2048]{1,0:T(8,128)(2,1)}), bf16[2048,2048]{1,0:T(8,128)(2,1)}) %all-gather.11.cloned.1.call-update) | async-done | bytes 8388624 | tf_op jit(solution)/shard_map/all_gather | solution.py:72
  433.7 16.5 %fusion.5 = bf16[512,2048]{1,0:T(8,128)(2,1)} fusion(bf16[2048,4096]{1,0:T(8,128)(2,1)} %constant_dynamic-update-slice_fusion, s32[]{:T(128)S(6)} %select_n.24, bf16[2048,2048]{1,0:T(8,128)(2,1)} %all-gather.11.cloned.1.call-done, f32[2048]{0:T(1024)S(1)} %convert_element_type.53, f32[512]{0:T(512)S(1)} %add_rsqrt_fusion, ...), kind=kOutput, calls=%fused_computation.11 | convolution fusion | flops 8600420352 | bytes 23078916 | tf_op jit(solution)/shard_map/dot_general | solution.py:77
  450.2 0.0 reduce-scatter.2.cloned.1.call-update
  450.3 45.4 %reduce-scatter.2.cloned.1.call-done = bf16[128,2048]{1,0:T(8,128)(2,1)} async-done(((bf16[512,2048]{1,0:T(8,128)(2,1)}), bf16[128,2048]{1,0:T(8,128)(2,1)}) %reduce-scatter.2.cloned.1.call-update) | async-done | bytes 524304 | tf_op jit(solution)/shard_map/reduce_scatter | solution.py:76
  495.7 2.3 add_convert_fusion
  (4 shorter events, 0.0 us)
Async XLA Ops:
  6.5 50.8 %all-gather.7.cloned.1.call-start = ((), (), s32[]{:S(2)}) async-start(), calls=%async_computation.2 | async-start | bytes 2621440 | tf_op jit(solution)/shard_map/all_gather | solution.py:44
  7.3 96.1 %all-gather.5.cloned.1.call-start = ((), (), s32[]{:S(2)}) async-start(), calls=%async_computation.1 | async-start | bytes 2621440 | tf_op jit(solution)/shard_map/all_gather | solution.py:39
  8.0 141.4 %all-gather.9.cloned.1.call-start = ((), (), s32[]{:S(2)}) async-start(), calls=%async_computation.3 | async-start | bytes 2621440 | tf_op jit(solution)/shard_map/all_gather | solution.py:63
  8.7 307.7 %all-reduce.4.cloned.1.call-start = ((), (), s32[]{:S(2)}) async-start(), calls=%async_computation.4 | async-start | bytes 4194304 | tf_op jit(solution)/shard_map/psum | solution.py:66
  14.8 88.6 %copy-start = (bf16[512,2048]{1,0:T(8,128)(2,1)S(1)}, bf16[512,2048]{1,0:T(8,128)(2,1)}, u32[]{:S(2)}) copy-start(bf16[512,2048]{1,0:T(8,128)(2,1)} %param.11) | copy-start | bytes 6291460
  153.9 162.5 %copy-start.4 = (bf16[2048]{0:T(1024)(128)(2,1)S(1)}, bf16[2048]{0:T(1024)(128)(2,1)}, u32[]{:S(2)}) copy-start(bf16[2048]{0:T(1024)(128)(2,1)} %param.19) | copy-start | bytes 12292
  153.9 279.8 %all-gather.11.cloned.1.call-start = ((), (), s32[]{:S(2)}) async-start(), calls=%async_computation.5 | async-start | bytes 10485760 | tf_op jit(solution)/shard_map/all_gather | solution.py:72
  154.5 341.2 %reduce-scatter.2.cloned.1.call-start = ((), (), s32[]{:S(2)}) async-start(), calls=%async_computation.6 | async-start | bytes 2621440 | tf_op jit(solution)/shard_map/reduce_scatter | solution.py:76
  154.6 49.3 %collective-permute-start = (bf16[2048,512]{1,0:T(8,128)(2,1)}, bf16[2048,512]{1,0:T(8,128)(2,1)S(1)}, u32[]{:S(2)}, u32[]{:S(2)}) collective-permute-start(bf16[2048,512]{1,0:T(8,128)(2,1)} %param.21), channel_id=1, source_target_pairs={{0,4},{4,8},{8,12},{12,0},{1,5},{5,9},{9,13},{13,1},{2,6},{6,10},{... | collective-permute-start | bytes 6291464 | tf_op jit(solution)/shard_map/ppermute | solution.py:15
  203.8 1.4 copy-start.2
  205.2 84.0 %collective-permute-start.1 = (bf16[2048,512]{1,0:T(8,128)(2,1)S(1)}, bf16[2048,512]{1,0:T(8,128)(2,1)}, u32[]{:S(2)}, u32[]{:S(2)}) collective-permute-start(bf16[2048,512]{1,0:T(8,128)(2,1)S(1)} %collective-permute-done), channel_id=1, source_target_pairs={{0,4},{4,8},{8,12},{12,0},{1,5},{5,9},{9,13},{13,1},{2,6},{6,10},{... | collective-permute-start | bytes 6291464 | tf_op jit(solution)/shard_map/ppermute | solution.py:15
  289.3 119.0 %collective-permute-start.2 = (bf16[2048,512]{1,0:T(8,128)(2,1)}, bf16[2048,512]{1,0:T(8,128)(2,1)}, u32[]{:S(2)}, u32[]{:S(2)}) collective-permute-start(bf16[2048,512]{1,0:T(8,128)(2,1)} %collective-permute-done.1), channel_id=1, source_target_pairs={{0,4},{4,8},{8,12},{12,0},{1,5},{5,9},{9,13},{13,1},{2,6},{6,10},{... | collective-permute-start | bytes 6291464 | tf_op jit(solution)/shard_map/ppermute | solution.py:15
  320.7 93.9 %copy-start.3 = (bf16[2048,512]{1,0:T(8,128)(2,1)S(1)}, bf16[2048,512]{1,0:T(8,128)(2,1)}, u32[]{:S(2)}) copy-start(bf16[2048,512]{1,0:T(8,128)(2,1)} %copy-done.2) | copy-start | bytes 6291460
  411.3 4.8 copy-start.1
Sparse Core Ops, SparseCore 0:
  8.9 48.3 all-gather.6
  58.9 44.4 all-gather.4
  105.0 44.4 all-gather.8
  154.0 50.1 all-reduce.3
  205.7 227.9 all-gather.10
  450.4 45.2 reduce-scatter.1
